TPU v7x, 128 devices: a whole 4x4x4 slice. The times are simulated.
128 devices in a mesh: rep: 2 (over z_hi), fs: 32 (over z_lo, y, x), tp: 2 (over core).
Axes of the slice: x: 4, y: 4, z: 4 (z_hi: 2, z_lo: 2; z = z_hi * 2 + z_lo), core: 2. Of those that a mesh axis runs over, the one named last changes fastest.
Arguments:
- hidden_in: bfloat16 [49152, 2048], P(('rep', 'fs', 'tp')), may hold values from -6 to 6
- norm_gain: float32 [2048], replicated, may hold values from 0.1 to 1.9
- up_weight: float32 [2048, 8192], P('fs', 'tp'), may hold values from -0.125 to 0.125
- up_scale: float32 [8192], P('tp'), may hold values from 0.5 to 2
- down_weight: float32 [8192, 2048], P('tp', 'fs'), may hold values from -0.0625 to 0.0625
- down_scale: float32 [2048], replicated, may hold values from 0.5 to 2
Outputs:
- layer_out: bfloat16 [49152, 2048], P(('rep', 'fs', 'tp'))
All inputs are finite; a program needn't handle non-finite values.
Results may differ from a plain program's by a relative error of at most 0.0085.
Values may be sent and summed in bfloat16 or wider, within the bound.
A program may use at most 128 MiB of HBM per device.

v0:
```python
import jax
import jax.numpy as jnp
from jax import lax
from jax.sharding import PartitionSpec as P


def in_blocks(shard, dim, size):
    before, after = (shard.shape[:dim], shard.shape[dim + 1 :])
    return jnp.moveaxis(shard.reshape(*before, size, -1, *after), dim, 0)


def sent_and_summed(shard, axis, dim):
    size = lax.axis_size(axis)
    parts = lax.all_to_all(in_blocks(shard, dim, size), axis, 0, 0, tiled=True)
    return jnp.sum(parts.astype(jnp.float32), axis=0)


def body(hidden_in, norm_gain, up_weight, up_scale, down_weight, down_scale):
    rows = hidden_in.astype(jnp.float32)
    normed = (
        rows * lax.rsqrt(jnp.mean(rows * rows, axis=1, keepdims=True) + 1e-06) * norm_gain
    ).astype(jnp.bfloat16)
    gathered = lax.all_gather(normed, "tp", axis=0, tiled=True)
    up_low = up_weight.astype(jnp.bfloat16)
    down_low = down_weight.astype(jnp.bfloat16)
    up_whole = lax.all_gather(up_low, "fs", axis=0, tiled=True)
    pre = jnp.dot(gathered, up_whole, preferred_element_type=jnp.float32)
    down_whole = lax.all_gather(down_low, "fs", axis=1, tiled=True)
    act = jnp.square(jnp.maximum(pre * up_scale, 0.0)).astype(jnp.bfloat16)
    summed = sent_and_summed(
        jnp.dot(act, down_whole, preferred_element_type=jnp.float32).astype(jnp.bfloat16), "tp", 0
    )
    return (summed * down_scale).astype(jnp.bfloat16)


def solution(mesh):
    placed = (P(("rep", "fs", "tp"), None), P(), P("fs", "tp"), P("tp"), P("tp", "fs"), P())
    return jax.shard_map(
        body, mesh=mesh, in_specs=placed, out_specs=P(("rep", "fs", "tp"), None), check_vma=False
    )
```

profile of v0, /device:TPU:1, one launch (start us, length us, event | category | flops | bytes accessed | tf_op | source)
XLA Modules:
  0.0 447.9 jit_solution(649375450214054075)
XLA Ops:
  6.5 0.0 copy-start
  6.5 0.0 all-gather.4.cloned.1.call-start
  6.5 1.9 fusion
  8.4 0.0 copy-start.1
  8.4 3.1 fusion.2
  11.5 0.0 copy-start.3
  11.5 0.0 all-gather.4.cloned.1.call-update
  11.5 0.0 all-gather.6.cloned.1.call-start
  11.6 0.0 copy-done
  11.6 0.9 convert_element_type.26
  12.5 0.0 all-gather.6.cloned.1.call-update
  12.5 0.0 all-gather.8.cloned.1.call-start
  12.5 0.0 copy-done.1
  12.5 0.9 convert_element_type.28
  13.4 0.0 all-gather.8.cloned.1.call-update
  13.4 16.7 %all-gather.4.cloned.1.call-done = bf16[768,2048]{1,0:T(8,128)(2,1)} async-done(((bf16[384,2048]{1,0:T(8,128)(2,1)}), bf16[768,2048]{1,0:T(8,128)(2,1)}) %all-gather.4.cloned.1.call-update) | async-done | bytes 3145744 | tf_op jit(solution)/shard_map/all_gather | solution.py:23
  30.1 192.8 %all-gather.6.cloned.1.call-done = bf16[2048,4096]{1,0:T(8,128)(2,1)} async-done(((bf16[64,4096]{1,0:T(8,128)(2,1)}), bf16[2048,4096]{1,0:T(8,128)(2,1)}) %all-gather.6.cloned.1.call-update) | async-done | bytes 16777232 | tf_op jit(solution)/shard_map/all_gather | solution.py:26
  222.9 0.0 copy-done.3
  222.9 19.2 %fusion.24 = bf16[768,4096]{1,0:T(8,128)(2,1)} fusion(f32[4096]{0:T(1024)S(1)} %copy-done.3, bf16[2048,4096]{1,0:T(8,128)(2,1)} %all-gather.6.cloned.1.call-done, bf16[768,2048]{1,0:T(8,128)(2,1)} %all-gather.4.cloned.1.call-done), kind=kOutput, calls=%bitcast_fusion.1.clone.1 | convolution fusion | flops 12897484800 | bytes 26230784 | tf_op jit(solution)/shard_map/dot_general | solution.py:27
  242.2 171.5 %all-gather.8.cloned.1.call-done = bf16[4096,2048]{0,1:T(8,128)(2,1)} async-done(((bf16[4096,64]{0,1:T(8,128)(2,1)}), bf16[4096,2048]{0,1:T(8,128)(2,1)}) %all-gather.8.cloned.1.call-update) | async-done | bytes 16777232 | tf_op jit(solution)/shard_map/all_gather | solution.py:28
  413.7 18.6 %convolution_convert_fusion = bf16[768,2048]{1,0:T(8,128)(2,1)S(1)} fusion(bf16[4096,2048]{0,1:T(8,128)(2,1)} %all-gather.8.cloned.1.call-done, bf16[768,4096]{1,0:T(8,128)(2,1)} %fusion.24), kind=kOutput, calls=%fused_computation.4 | convolution fusion | flops 12886474752 | bytes 26214400 | tf_op jit(solution)/shard_map/dot_general | solution.py:31
  432.2 6.9 %all_to_all.5 = bf16[2,384,2048]{2,1,0:T(8,128)(2,1)S(1)} all-to-all(bf16[2,384,2048]{2,1,0:T(8,128)(2,1)S(1)} %bitcast.24), channel_id=1, replica_groups=mesh['rep'=2,'fs'=32,'tp'=2] {'tp'}, dimensions={0} | all-to-all | bytes 6291456 | tf_op jit(solution)/shard_map/all_to_all | solution.py:14
  439.2 0.0 copy-start.2
  439.2 0.7 convert_reduce_fusion
  439.9 0.0 copy-done.2
  439.9 1.5 multiply_convert_fusion.1
  (1 shorter events, 0.0 us)
Async XLA Ops:
  6.5 5.0 %copy-start = (f32[64,4096]{1,0:T(8,128)S(1)}, f32[64,4096]{1,0:T(8,128)}, u32[]{:S(2)}) copy-start(f32[64,4096]{1,0:T(8,128)} %param.8) | copy-start | bytes 3145732
  6.5 23.6 %all-gather.4.cloned.1.call-start = ((), (), s32[]{:S(2)}) async-start(), calls=%async_computation.1 | async-start | bytes 4718592 | tf_op jit(solution)/shard_map/all_gather | solution.py:23
  8.4 4.1 copy-start.1
  11.5 211.4 %copy-start.3 = (f32[4096]{0:T(1024)S(1)}, f32[4096]{0:T(1024)}, u32[]{:S(2)}) copy-start(f32[4096]{0:T(1024)} %param.9) | copy-start | bytes 49156
  11.5 211.4 %all-gather.6.cloned.1.call-start = ((), (), s32[]{:S(2)}) async-start(), calls=%async_computation.2 | async-start | bytes 17301504 | tf_op jit(solution)/shard_map/all_gather | solution.py:26
  12.5 401.2 %all-gather.8.cloned.1.call-start = ((), (), s32[]{:S(2)}) async-start(), calls=%async_computation.3 | async-start | bytes 17301504 | tf_op jit(solution)/shard_map/all_gather | solution.py:28
  439.2 0.7 copy-start.2
Sparse Core Ops, SparseCore 0:
  11.7 18.4 all-gather.3
  31.8 191.0 all-gather.5
  224.6 189.0 all-gather.7
where the time goes:
time: 448 us
  waiting for transfers between devices  381 us (85%)
  matrix products  37.8 us (8%)
  between operations  13.2 us (3%)
  other arithmetic  8.87 us (2%)
  blocking collectives  6.92 us (2%)
    all_gather x1, waiting for transfers between devices, body(): up_whole = lax.all_gather(up_low, 'fs', axis=0, tiled=True)  193 us
    all_gather x1, waiting for transfers between devices, body(): down_whole = lax.all_gather(down_low, 'fs', axis=1, tiled=True)  172 us
    dot_general x1, matrix products, body(): pre = jnp.dot(gathered, up_whole, preferred_element_type=jnp.float32)  19.2 us
    dot_general x1, matrix products, body(): jnp.dot(act, down_whole, preferred_element_type=jnp.float32)  18.6 us
    all_gather x1, waiting for transfers between devices, body(): gathered = lax.all_gather(normed, 'tp', axis=0, tiled=True)  16.7 us
  transfers between devices with their start and end apart: 3, of which 3 were waited for; matrix products, arithmetic and copies ran while one was open for 5% of the time, Pallas kernels for 0%

commit v1 on v0

v1 whole, which is shorter than its diff:
```python
import jax
import jax.numpy as jnp
from jax import lax
from jax.experimental import pallas as pl
from jax.experimental.pallas import tpu as pltpu
from jax.sharding import PartitionSpec as P

F32, BF16 = jnp.float32, jnp.bfloat16
ROWS, D, Q, GROUP, BLOCK = 384, 2048, 2048, 256, 64
HALF = Q // 2
STEP = ((1, 0, 0), (3, 0, 0), (0, 1, 0), (0, 3, 0), (0, 0, 1))
ORDER = (
    ((0, 0), (0, 1), (1, 0), (3, 0), (1, 1), (3, 1), (2, 0), (2, 1)),
    ((0, 0), (0, 1), (3, 0), (1, 0), (3, 1), (1, 1), (2, 0), (2, 1)),
)
PLAN = (
    (0,0,0,1,0,0,0), (0,0,1,1,0,0,0), (0,0,1,3,0,0,1), (0,0,0,3,0,0,1), (0,0,1,0,1,0,2), (0,0,0,0,1,0,2),
    (0,0,0,0,3,0,3), (0,0,1,0,3,0,3), (0,0,0,0,0,1,4), (0,0,1,0,0,1,4), (0,1,1,1,0,0,0), (0,1,0,3,0,0,1),
    (0,1,0,0,3,0,3), (0,1,0,0,0,1,4), (0,0,0,1,1,0,2), (0,0,0,1,0,1,0), (0,0,0,3,0,1,1), (0,0,0,0,1,1,2),
    (0,0,1,3,3,0,3), (0,0,1,0,1,1,4), (1,0), (0,1,0,1,0,0,0), (0,0,1,2,0,0,1), (0,0,0,0,2,0,2), (0,0,1,0,3,1,3),
    (0,0,1,1,0,1,4), (0,0,0,2,1,0,0), (0,0,1,3,1,0,1), (0,0,0,1,2,0,2), (0,0,0,3,3,0,3), (0,0,0,1,1,1,4), (1,1),
    (0,0,1,1,1,1,0), (0,0,0,2,0,1,1), (0,0,1,0,2,1,2), (0,0,0,1,3,0,3), (0,0,1,3,3,1,4), (1,2), (0,0,1,1,3,1,0),
    (0,0,0,3,1,1,1), (0,0,1,2,1,0,2), (0,0,1,3,2,0,3), (0,0,1,2,0,1,4), (0,0,0,2,2,0,0), (0,0,0,2,3,0,1),
    (0,0,0,1,2,1,2), (0,0,0,2,0,0,3), (0,0,1,3,1,1,4), (1,3), (0,1,1,2,0,0,0), (0,0,1,2,3,0,1), (0,0,1,3,0,1,2),
    (0,0,0,0,3,1,3), (0,0,0,1,3,1,4), (1,4), (0,0,1,0,2,0,0), (0,0,1,1,1,0,1), (0,0,1,2,1,1,2), (0,0,0,3,3,1,3),
    (0,0,0,3,1,0,4), (2,0,0), (0,0,0,3,2,0,0), (0,0,0,2,1,1,1), (0,0,1,2,2,0,2), (0,0,0,2,3,1,3), (0,0,1,1,3,0,4),
    (2,0,1), (1,5), (2,1,0), (0,0,0,2,2,1,0), (0,1,0,2,0,0,1), (0,0,1,1,2,1,2), (0,0,1,2,3,1,3), (0,0,0,0,2,1,4),
    (2,1,1), (1,6), (2,2,0), (0,0,1,1,2,0,0), (0,1,0,3,0,1,1), (0,0,1,2,2,1,2), (0,0,0,3,2,1,3), (0,0,1,3,2,1,4),
    (2,2,1), (2,3,0), (0,1,0,1,0,1,0), (0,1,1,3,0,0,1), (0,1,0,3,1,0,2), (0,1,1,2,3,0,3), (0,1,1,2,0,1,4), (2,3,1),
    (1,7), (2,4,0), (2,4,1), (0,1,0,1,3,0,0), (0,1,0,2,1,0,2), (0,1,0,3,3,0,3), (0,1,1,0,0,1,4), (2,5,0), (2,5,1),
    (0,1,0,2,0,1,1), (2,6,0), (0,1,1,1,1,0,2), (0,1,0,2,3,0,3), (2,6,1), (2,7,0), (0,1,1,3,3,0,0), (0,1,1,1,0,1,1),
    (0,1,1,3,0,1,4), (2,7,1), (0,1,0,0,1,0,0), (0,1,1,1,3,0,1), (0,1,1,3,1,0,2), (0,1,1,0,3,0,3), (0,1,1,2,3,1,4),
    (3,0), (4,0), (0,1,0,1,1,0,1), (0,1,0,2,1,1,2), (0,1,0,0,3,1,3), (0,1,0,3,3,1,4), (5,0), (0,1,1,2,1,0,0), (3,1),
    (0,1,0,3,2,0,2), (0,1,1,0,3,1,3), (0,1,1,3,3,1,4), (4,1), (5,1), (0,1,1,0,1,0,0), (0,1,1,1,3,1,1), (3,2),
    (0,1,1,0,1,1,2), (0,1,1,0,2,0,3), (0,1,0,0,1,1,4), (4,2), (5,2), (6,0), (0,1,0,1,3,1,0), (0,1,0,2,3,1,1),
    (0,1,0,3,1,1,0), (0,1,0,1,2,0,2), (0,1,0,0,2,1,3), (0,1,1,1,1,1,4), (0,1,0,2,2,0,1), (3,3), (0,1,1,3,1,1,2),
    (0,1,1,2,2,0,3), (0,1,1,2,1,1,4), (6,1), (4,3), (5,3), (0,1,0,1,1,1,0), (0,1,1,3,2,0,1), (3,4), (0,1,1,1,2,0,0),
    (0,1,1,0,2,1,3), (4,4), (5,4), (6,2), (0,1,0,0,2,0,1), (0,1,0,2,2,1,4), (0,1,0,3,2,1,1), (0,1,1,1,2,1,3),
    (0,1,0,1,2,1,2), (0,1,1,3,2,1,2), (0,1,1,2,2,1,4), (3,5), (4,5), (5,5), (6,3), (3,6), (4,6), (5,6), (6,4), (3,7),
    (4,7), (6,5), (5,7), (6,6), (6,7),
)


def kernel(hidden, gain, up, up_scale, down, down_scale, out, hbuf, ubuf, dbuf, w, x, acc, act, pbuf, sibp, mine, own,
           zbuf, zrecv, obuf, in_sem, ag_send, ag_recv, tok_send, tok_recv, par_send, par_recv, out_sem):
    rep, fs, core = lax.axis_index("rep"), lax.axis_index("fs"), lax.axis_index("tp")
    lo, yy, xx = fs // 16, (fs // 4) % 4, fs % 4
    turn = 1 + 2 * core

    def at(px, py, plo):
        return (plo * 4 + py) * 4 + px

    def neighbour(d):
        dx, dy, dz = STEP[d]
        return {"fs": at((xx + turn * dx) % 4, (yy + dy) % 4, (lo + dz) % 2)}

    sibling = {"tp": 1 - core}
    across = {"rep": 1 - rep, "fs": at(xx, yy, 1 - lo)}

    loads = [
        pltpu.make_async_copy(up.at[:, pl.ds(pl.multiple_of(rep * Q, Q), Q)], ubuf, in_sem.at[0]),
        pltpu.make_async_copy(hidden, hbuf, in_sem.at[1]),
        pltpu.make_async_copy(down.at[:, pl.ds(pl.multiple_of(rep * Q, Q), Q)], dbuf, in_sem.at[2]),
    ]
    for load in loads:
        load.start()
    barrier = pltpu.get_barrier_semaphore()
    for peer in [neighbour(d) for d in range(5)] + [sibling, across]:
        pl.semaphore_signal(barrier, inc=1, device_id=peer, device_id_type=pl.DeviceIdType.MESH)

    me_rows = pl.ds(pl.multiple_of(fs * BLOCK, BLOCK), BLOCK)
    loads[0].wait()
    w[0, me_rows, :] = ubuf[...].astype(BF16)
    loads[2].wait()
    w[1, me_rows, :] = dbuf[...].astype(BF16)
    pl.semaphore_wait(barrier, 7)

    def block_rows(o):
        return pl.ds(pl.multiple_of(at((xx + 4 - (turn * o[0]) % 4) % 4, (yy + 4 - o[1]) % 4, (lo + o[2]) % 2) * BLOCK, BLOCK), BLOCK)

    def remote(src, dst, send, recv, peer):
        return pltpu.make_async_remote_copy(src_ref=src, dst_ref=dst, send_sem=send, recv_sem=recv, device_id=peer,
                                            device_id_type=pl.DeviceIdType.MESH)

    def number(phase, half, o):
        return ((phase * 2 + half) * 2 + o[2]) * 16 + o[1] * 4 + o[0]

    waited = set()

    def block_copy(phase, half, o, d):
        s = STEP[d]
        held = ((o[0] - s[0]) % 4, (o[1] - s[1]) % 4, (o[2] - s[2]) % 2)
        ref = w.at[phase, block_rows(held), pl.ds(half * HALF, HALF)]
        return remote(ref, ref, ag_send.at[phase], ag_recv.at[number(phase, half, o)], neighbour(d))

    def need(phase, half, o):
        if o != (0, 0, 0) and (phase, half, o) not in waited:
            waited.add((phase, half, o))
            ref = w.at[phase, block_rows(o), pl.ds(half * HALF, HALF)]
            remote(ref, ref, ag_send.at[phase], ag_recv.at[number(phase, half, o)], sibling).wait_recv()

    def send(phase, half, o, d):
        s = STEP[d]
        held = ((o[0] - s[0]) % 4, (o[1] - s[1]) % 4, (o[2] - s[2]) % 2)
        need(phase, half, held)
        block_copy(phase, half, o, d).start()

    def need_group(phase, g):
        y, z = ORDER[phase][g]
        for half in range(2):
            for a in range(4):
                need(phase, half, (a, y, z))

    def group(phase, g, far=0):
        y, z = ORDER[phase][g]
        return ((lo + far + z) % 2) * 4 + (yy + 4 - y) % 4

    def columns(a):
        return pl.ds(pl.multiple_of(a * GROUP, GROUP), GROUP)

    sib_rows, sib_far_rows, my_rows, far_rows = (pl.ds(i * ROWS, ROWS) for i in range(4))

    def token_far(g):
        a = group(0, g, 1)
        return remote(x.at[a, my_rows], x.at[a, far_rows], tok_send.at[0], tok_recv.at[0, g], across)

    def token_far_in(g):
        a = group(0, g)
        return remote(x.at[a, my_rows], x.at[a, far_rows], tok_send.at[0], tok_recv.at[0, g], across)

    def token_near(g):
        a = group(0, g)
        return remote(x.at[a, my_rows], x.at[a, sib_rows], tok_send.at[1], tok_recv.at[1, g], sibling)

    def token_relay(g):
        a = group(0, g)
        return remote(x.at[a, far_rows], x.at[a, sib_far_rows], tok_send.at[2], tok_recv.at[2, g], sibling)

    def near_part(g):
        return remote(pbuf.at[g], sibp.at[g], par_send.at[0], par_recv.at[0, g], sibling)

    def far_part(g):
        return remote(zbuf.at[g], zrecv.at[g], par_send.at[1], par_recv.at[1, g], across)

    plan = list(PLAN)
    while plan[0][0] == 0:
        send(plan[0][1], plan[0][2], plan[0][3:6], plan[0][6])
        plan.pop(0)

    loads[1].wait()

    @pl.loop(0, ROWS // 32)
    def _(i):
        rows = hbuf[pl.ds(i * 32, 32), :].astype(F32)
        inv = lax.rsqrt(jnp.mean(rows * rows, axis=1, keepdims=True) + 1e-06)
        normed = (rows * inv * gain[...]).astype(BF16)
        for a in range(8):
            x[a, pl.ds(2 * ROWS + i * 32, 32), :] = normed[:, a * GROUP:(a + 1) * GROUP]

    for g in range(8):
        token_far(g).start()
        token_near(g).start()

    half_scale = up_scale.at[:, pl.ds(pl.multiple_of(rep * Q, Q), Q)]

    def up_product(g, part):
        if part == 0:
            need_group(0, g)
            token_near(g).wait_recv()
            token_relay(g).wait_recv()
        a = group(0, g)

        @pl.loop(part * 4, part * 4 + 4)
        def _(n):
            tokens = x[a]
            total = jnp.dot(tokens, w[0, columns(a), columns(n)], preferred_element_type=F32)
            if g > 0:
                total = total + acc[n]
            if g < 7:
                acc[n] = total
            else:
                act[:, columns(n)] = jnp.square(jnp.maximum(total * half_scale[:, columns(n)], 0.0)).astype(BF16)

    def product(rows, a):
        return lax.dot_general(act[rows, :], w[1, columns(a), :], (((1,), (1,)), ((), ())), preferred_element_type=F32)

    def down_first(g):
        need_group(1, g)
        a = group(1, g)

        @pl.loop(0, 2)
        def _(m):
            rows = pl.ds(pl.multiple_of(m * ROWS, ROWS), ROWS)
            pbuf[g, rows, :] = product(rows, a).astype(BF16)

        near_part(g).start()

    def down_second(g):
        a = group(1, g)

        @pl.loop(0, 2)
        def _(m):
            own[m] = product(pl.ds(pl.multiple_of((m + 2) * ROWS, ROWS), ROWS), a)

    def chip_sum(g):
        a = group(1, g)
        near_part(g).wait_recv()
        zbuf[g] = (own[1] + sibp[g, pl.ds(ROWS, ROWS), :].astype(F32)).astype(BF16)
        far_part(g).start()
        mine[a] = own[0] + sibp[g, pl.ds(0, ROWS), :].astype(F32)

    def out_copy(g):
        return pltpu.make_async_copy(obuf.at[g], out.at[:, columns(group(1, g, 1))], out_sem.at[g])

    def output(g):
        a = group(1, g, 1)
        far_part(g).wait_recv()
        obuf[g] = ((mine[a] + zrecv[g].astype(F32)) * down_scale[:, columns(a)]).astype(BF16)
        out_copy(g).start()

    for step in plan:
        kind, arg = step[0], step[1]
        if kind == 0:
            send(arg, step[2], step[3:6], step[6])
        elif kind == 1:
            token_far_in(arg).wait_recv()
            token_relay(arg).start()
        elif kind == 2:
            up_product(arg, step[2])
        elif kind == 3:
            down_first(arg)
        elif kind == 4:
            down_second(arg)
        elif kind == 5:
            chip_sum(arg)
        else:
            output(arg)

    for phase in range(2):
        sent = w.at[phase, pl.ds(0, 31 * BLOCK), :]
        remote(sent, sent, ag_send.at[phase], ag_recv.at[0], sibling).wait_send()
    for i in range(3):
        sent = x.at[:, pl.ds(0, ROWS)]
        remote(sent, sent, tok_send.at[i], tok_recv.at[0, 0], sibling).wait_send()
    remote(pbuf, pbuf, par_send.at[0], par_recv.at[0, 0], sibling).wait_send()
    remote(zbuf, zbuf, par_send.at[1], par_recv.at[0, 0], sibling).wait_send()
    for g in range(8):
        out_copy(g).wait()


def body(hidden_in, norm_gain, up_weight, up_scale, down_weight, down_scale):
    vmem, anywhere = pl.BlockSpec(memory_space=pltpu.VMEM), pl.BlockSpec(memory_space=pl.ANY)
    dma = pltpu.SemaphoreType.DMA
    return pl.pallas_call(
        kernel,
        out_shape=jax.ShapeDtypeStruct((ROWS, D), BF16),
        in_specs=[anywhere, vmem, anywhere, vmem, anywhere, vmem],
        out_specs=anywhere,
        scratch_shapes=[
            pltpu.VMEM((ROWS, D), BF16),
            pltpu.VMEM((BLOCK, Q), F32),
            pltpu.VMEM((BLOCK, Q), F32),
            pltpu.VMEM((2, D, Q), BF16),
            pltpu.VMEM((8, 4 * ROWS, GROUP), BF16),
            pltpu.VMEM((8, 4 * ROWS, GROUP), F32),
            pltpu.VMEM((4 * ROWS, Q), BF16),
            pltpu.VMEM((8, 2 * ROWS, GROUP), BF16),
            pltpu.VMEM((8, 2 * ROWS, GROUP), BF16),
            pltpu.VMEM((8, ROWS, GROUP), F32),
            pltpu.VMEM((2, ROWS, GROUP), F32),
            pltpu.VMEM((8, ROWS, GROUP), BF16),
            pltpu.VMEM((8, ROWS, GROUP), BF16),
            pltpu.VMEM((8, ROWS, GROUP), BF16),
            dma((3,)),
            dma((2,)),
            dma((128,)),
            dma((3,)),
            dma((3, 8)),
            dma((2,)),
            dma((2, 8)),
            dma((8,)),
        ],
        compiler_params=pltpu.CompilerParams(collective_id=0, has_side_effects=True, vmem_limit_bytes=67043328),
        name="ffn",
    )(hidden_in, norm_gain.reshape(1, -1), up_weight, up_scale.reshape(1, -1), down_weight.T, down_scale.reshape(1, -1))


def solution(mesh):
    placed = (P(("rep", "fs", "tp"), None), P(), P("fs", "tp"), P("tp"), P("tp", "fs"), P())
    return jax.shard_map(
        body, mesh=mesh, in_specs=placed, out_specs=P(("rep", "fs", "tp"), None), check_vma=False
    )
```

time: 448 us -> 111 us (0.25)
  waiting for transfers between devices: 381 us -> 0 us
  Pallas kernels: 0 us -> 108 us
  matrix products: 37.8 us -> 0 us
  between operations: 13.2 us -> 0.01 us
  other arithmetic: 8.87 us -> 0 us
  blocking collectives: 6.92 us -> 0 us
    all_gather x3 -> x0, waiting for transfers between devices: 381 us -> none  [the longest x1 193 us: body(): up_whole = lax.all_gather(up_low, 'fs', axis=0, tiled=True)]
    pallas_call x0 -> x1, Pallas kernels: none -> 108 us  [body(): pl.pallas_call(kernel, out_shape=jax.ShapeDtypeStruct((ROWS, D), BF16), i...]
    dot_general x2 -> x0, matrix products: 37.8 us -> none  [the longest x1 19.2 us: body(): pre = jnp.dot(gathered, up_whole, preferred_element_type=jnp.float32)]
    all_to_all x1 -> x0, blocking collectives: 6.92 us -> none  [sent_and_summed(): parts = lax.all_to_all(in_blocks(shard, dim, size), axis, 0, 0, tiled=True)]
    convert_element_type x4 -> x0, other arithmetic: 6.26 us -> none  [the longest x1 3.07 us: body(): normed = (rows * lax.rsqrt(jnp.mean(rows * rows, axis=1, keepdims=True) +...]
  transfers between devices with their start and end apart: 3 -> 0, of which waited for: 3 -> 0; matrix products, arithmetic and copies ran while one was open for 5% -> 0% of each run, Pallas kernels for 0% -> 0%
where the time goes in v1:
time: 111 us; the launch traced here: 110 us
  Pallas kernels  108 us (97%)
  local copies, waits for them, and re-layouts  2.73 us (2%)
    pallas_call x1, Pallas kernels, body(): pl.pallas_call(kernel, out_shape=jax.ShapeDtypeStruct((ROWS, D), BF16), i...  108 us
    unnamed x1, local copies, waits for them, and re-layouts  2.73 us

profile of v1, /device:TPU:1, one launch (start us, length us, event | category | flops | bytes accessed | tf_op | source)
XLA Modules:
  0.0 110.4 jit_solution(7224138270100449746)
XLA Ops:
  0.0 107.7 %ffn.1 = bf16[384,2048]{1,0:T(8,128)(2,1)} custom-call(bf16[384,2048]{1,0:T(8,128)(2,1)} %hidden.1, f32[1,2048]{1,0:T(1,128)} %bitcast.6, f32[64,4096]{1,0:T(8,128)} %up.1, f32[1,4096]{1,0:T(1,128)} %bitcast.5, f32[64,4096]{1,0:T(8,128)} %bitcast.4, f32[1,2048]{1,0:T(1,128)} %bitcast.7), custom_call_target="tpu_custom_call" | custom-call | tf_op jit(solution)/shard_map/ffn/pallas_call | solution.py:254
  107.7 2.7 %copy.8 = bf16[384,2048]{1,0:T(8,128)(2,1)} copy(bf16[384,2048]{1,0:T(8,128)(2,1)} %ffn.1) | data formatting | bytes 3145728

commit v2 on v1

v2 whole, which is shorter than its diff:
```python
import jax
import jax.numpy as jnp
from jax import lax
from jax.experimental import pallas as pl
from jax.experimental.pallas import tpu as pltpu
from jax.sharding import PartitionSpec as P

F32, BF16 = jnp.float32, jnp.bfloat16
ROWS, D, Q, GROUP, BLOCK = 384, 2048, 2048, 256, 64
HALF, WIDE = Q // 2, Q // 2
STEP = ((1, 0, 0), (3, 0, 0), (0, 1, 0), (0, 3, 0), (0, 0, 1))
ORDER = (
    ((0, 0), (0, 1), (1, 0), (3, 0), (1, 1), (3, 1), (2, 0), (2, 1)),
    ((0, 0), (0, 1), (3, 0), (1, 0), (3, 1), (1, 1), (2, 0), (2, 1)),
)
PLAN = (
    (0,0,0,1,0,0,0), (0,0,1,1,0,0,0), (0,0,1,3,0,0,1), (0,0,0,3,0,0,1), (0,0,1,0,1,0,2), (0,0,0,0,1,0,2),
    (0,0,1,0,3,0,3), (0,0,0,0,3,0,3), (0,0,0,0,0,1,4), (0,1,1,0,0,1,4), (0,1,0,1,0,0,0), (0,1,0,3,0,0,1),
    (0,1,1,0,3,0,3), (0,0,0,1,1,0,2), (0,0,1,3,0,1,4), (0,0,0,1,0,1,0), (0,0,1,2,0,0,1), (0,0,1,3,1,0,2),
    (0,0,0,1,3,0,3), (0,0,1,0,1,1,4), (0,0,0,2,0,0,0), (0,0,0,3,1,0,1), (0,0,1,1,1,0,2), (1,0), (0,0,1,0,2,0,3),
    (0,0,1,1,0,1,4), (0,0,0,2,1,0,0), (0,0,1,2,0,1,1), (0,0,0,1,2,0,2), (0,0,1,3,3,0,3), (0,0,0,3,0,1,4), (1,1),
    (0,0,1,1,1,1,0), (0,0,1,2,1,0,1), (0,0,0,1,1,1,2), (0,0,1,0,0,1,3), (0,0,0,0,3,1,4), (2,0,0), (0,0,1,1,2,0,0),
    (0,1,1,3,0,0,1), (0,0,0,3,2,0,2), (0,0,1,2,3,0,3), (0,0,0,3,1,1,4), (1,2), (2,0,1), (0,0,0,2,0,1,0),
    (0,0,0,0,2,0,1), (0,0,1,2,1,1,2), (0,0,0,3,3,1,3), (0,0,0,2,1,1,4), (1,3), (0,0,0,2,3,0,0), (0,1,0,2,0,0,1),
    (0,0,1,0,2,1,2), (0,0,1,1,3,1,3), (0,0,0,1,3,1,4), (0,0,0,0,1,1,0), (0,0,1,1,3,0,1), (1,4), (0,0,0,3,3,0,2),
    (0,0,0,0,2,1,3), (0,0,1,1,2,1,4), (2,1,0), (0,0,1,3,1,1,0), (0,1,1,2,0,0,1), (0,0,1,2,2,0,2), (0,0,0,2,3,1,3),
    (0,0,1,2,3,1,4), (2,1,1), (1,5), (2,2,0), (0,1,1,1,3,0,0), (0,0,1,3,2,1,1), (0,0,1,0,3,1,2), (0,0,1,3,2,0,3),
    (0,0,1,3,3,1,4), (2,2,1), (2,3,0), (0,0,0,1,2,1,0), (0,1,1,3,0,1,1), (0,0,0,2,2,1,2), (0,0,0,2,2,0,3),
    (0,1,0,3,0,1,4), (1,6), (2,3,1), (2,4,0), (0,0,1,2,2,1,0), (0,1,1,1,0,0,1), (0,0,0,3,2,1,2), (0,1,0,3,3,0,3),
    (0,1,0,1,0,1,4), (2,4,1), (1,7), (2,5,0), (0,1,1,2,3,0,0), (0,1,0,3,1,0,2), (0,1,0,2,3,0,3), (0,1,1,0,3,1,4),
    (2,5,1), (0,1,1,2,0,1,1), (2,6,0), (0,1,0,0,0,1,0), (0,1,0,2,0,1,1), (0,1,1,3,1,0,2), (0,1,0,0,3,0,3), (2,6,1),
    (0,1,1,1,0,1,4), (2,7,0), (0,1,1,1,1,0,2), (0,1,1,3,3,0,3), (0,1,0,3,3,1,4), (3,0), (0,1,0,0,1,0,0),
    (0,1,0,1,3,0,1), (2,7,1), (0,1,1,1,3,1,0), (0,1,0,2,1,0,1), (0,1,1,2,1,0,2), (0,1,1,3,3,1,3), (0,1,0,3,1,1,4),
    (4,0), (5,0), (0,1,1,2,1,1,2), (0,1,0,2,3,1,3), (3,1), (6,0), (5,1), (0,1,0,1,1,0,0), (0,1,0,0,3,1,0),
    (0,1,1,0,1,0,1), (0,1,1,1,2,0,2), (0,1,0,0,2,0,3), (0,1,0,1,3,1,4), (4,1), (3,2), (6,1), (5,2), (0,1,0,0,1,1,0),
    (0,1,1,2,3,1,1), (0,1,1,3,2,0,2), (0,1,0,1,2,0,3), (0,1,0,2,1,1,4), (4,2), (7,0), (6,2), (0,1,1,1,1,1,1),
    (0,1,0,1,1,1,4), (0,1,1,2,2,1,2), (3,3), (0,1,1,3,1,1,0), (0,1,0,2,2,1,3), (0,1,1,0,1,1,4), (5,3),
    (0,1,0,3,2,0,1), (4,3), (0,1,1,2,2,0,3), (7,1), (3,4), (0,1,1,0,2,0,1), (0,1,1,1,2,1,4), (6,3), (5,4),
    (0,1,0,2,2,0,0), (0,1,0,0,2,1,2), (4,4), (0,1,1,3,2,1,4), (6,4), (7,2), (0,1,0,3,2,1,0), (0,1,0,1,2,1,1),
    (0,1,1,0,2,1,2), (3,5), (5,5), (4,5), (3,6), (6,5), (5,6), (4,6), (3,7), (6,6), (5,7), (4,7), (7,3), (7,4),
    (6,7), (7,5), (7,6), (7,7),
)


def kernel(hidden, gain, up, up_scale, down, down_scale, out, hbuf, ubuf, dbuf, w, x, acc, act, pbuf, sibp, own, zbuf, zrecv,
           in_sem, ag_send, ag_recv, tok_send, tok_recv, par_send, par_recv):
    rep, fs, core = lax.axis_index("rep"), lax.axis_index("fs"), lax.axis_index("tp")
    lo, yy, xx = fs // 16, (fs // 4) % 4, fs % 4
    turn = 1 + 2 * core

    def at(px, py, plo):
        return (plo * 4 + py) * 4 + px

    def neighbour(d):
        dx, dy, dz = STEP[d]
        return {"fs": at((xx + turn * dx) % 4, (yy + dy) % 4, (lo + dz) % 2)}

    sibling = {"tp": 1 - core}
    across = {"rep": 1 - rep, "fs": at(xx, yy, 1 - lo)}

    loads = [
        pltpu.make_async_copy(up.at[:, pl.ds(pl.multiple_of(rep * Q, Q), Q)], ubuf, in_sem.at[0]),
        pltpu.make_async_copy(hidden, hbuf, in_sem.at[1]),
        pltpu.make_async_copy(down.at[:, pl.ds(pl.multiple_of(rep * Q, Q), Q)], dbuf, in_sem.at[2]),
    ]
    for load in loads:
        load.start()
    barrier = pltpu.get_barrier_semaphore()
    for peer in [neighbour(d) for d in range(5)] + [sibling, across]:
        pl.semaphore_signal(barrier, inc=1, device_id=peer, device_id_type=pl.DeviceIdType.MESH)

    me_rows = pl.ds(pl.multiple_of(fs * BLOCK, BLOCK), BLOCK)
    loads[0].wait()
    w[0, me_rows, :] = ubuf[...].astype(BF16)
    loads[2].wait()
    w[1, me_rows, :] = dbuf[...].astype(BF16)
    pl.semaphore_wait(barrier, 7)

    def block_rows(o):
        return pl.ds(pl.multiple_of(at((xx + 4 - (turn * o[0]) % 4) % 4, (yy + 4 - o[1]) % 4, (lo + o[2]) % 2) * BLOCK, BLOCK), BLOCK)

    def remote(src, dst, send, recv, peer):
        return pltpu.make_async_remote_copy(src_ref=src, dst_ref=dst, send_sem=send, recv_sem=recv, device_id=peer,
                                            device_id_type=pl.DeviceIdType.MESH)

    def number(phase, half, o):
        return ((phase * 2 + half) * 2 + o[2]) * 16 + o[1] * 4 + o[0]

    waited = set()

    def block_copy(phase, half, o, d):
        s = STEP[d]
        held = ((o[0] - s[0]) % 4, (o[1] - s[1]) % 4, (o[2] - s[2]) % 2)
        ref = w.at[phase, block_rows(held), pl.ds(half * HALF, HALF)]
        return remote(ref, ref, ag_send.at[phase], ag_recv.at[number(phase, half, o)], neighbour(d))

    def need(phase, half, o):
        if o != (0, 0, 0) and (phase, half, o) not in waited:
            waited.add((phase, half, o))
            ref = w.at[phase, block_rows(o), pl.ds(half * HALF, HALF)]
            remote(ref, ref, ag_send.at[phase], ag_recv.at[number(phase, half, o)], sibling).wait_recv()

    def send(phase, half, o, d):
        s = STEP[d]
        held = ((o[0] - s[0]) % 4, (o[1] - s[1]) % 4, (o[2] - s[2]) % 2)
        need(phase, half, held)
        block_copy(phase, half, o, d).start()

    def need_group(phase, g):
        y, z = ORDER[phase][g]
        for half in range(2):
            for a in range(4):
                need(phase, half, (a, y, z))

    def group(phase, g, far=0):
        y, z = ORDER[phase][g]
        return ((lo + far + z) % 2) * 4 + (yy + 4 - y) % 4

    def columns(a):
        return pl.ds(pl.multiple_of(a * GROUP, GROUP), GROUP)

    sib_far_rows, far_rows, sib_rows, my_rows = (pl.ds(i * ROWS, ROWS) for i in range(4))

    def token_far(g):
        a = group(0, g, 1)
        return remote(x.at[a, my_rows], x.at[a, far_rows], tok_send.at[0], tok_recv.at[0, g], across)

    def token_far_in(g):
        a = group(0, g)
        return remote(x.at[a, my_rows], x.at[a, far_rows], tok_send.at[0], tok_recv.at[0, g], across)

    def token_near(g):
        a = group(0, g)
        return remote(x.at[a, my_rows], x.at[a, sib_rows], tok_send.at[1], tok_recv.at[1, g], sibling)

    def token_relay(g):
        a = group(0, g)
        return remote(x.at[a, far_rows], x.at[a, sib_far_rows], tok_send.at[2], tok_recv.at[2, g], sibling)

    def near_part(g, i):
        return remote(pbuf.at[2 * g + i, 0], sibp.at[g, i], par_send.at[0], par_recv.at[i, g], sibling)

    def far_part(g):
        return remote(zbuf.at[g], zrecv.at[g], par_send.at[1], par_recv.at[2, g], across)

    plan = list(PLAN)
    while plan[0][0] == 0 and STEP[plan[0][6]] == tuple(plan[0][3:6]):
        send(plan[0][1], plan[0][2], plan[0][3:6], plan[0][6])
        plan.pop(0)
    loads[1].wait()

    @pl.loop(0, ROWS // 32)
    def _(i):
        rows = hbuf[pl.ds(i * 32, 32), :].astype(F32)
        inv = lax.rsqrt(jnp.mean(rows * rows, axis=1, keepdims=True) + 1e-06)
        normed = (rows * inv * gain[...]).astype(BF16)
        for a in range(8):
            x[a, pl.ds(3 * ROWS + i * 32, 32), :] = normed[:, a * GROUP:(a + 1) * GROUP]

    for g in range(8):
        token_far(g).start()
    for g in range(8):
        token_near(g).start()

    half_scale = up_scale.at[:, pl.ds(pl.multiple_of(rep * Q, Q), Q)]

    def up_product(g, part):
        need_group(0, g)
        if part == 0:
            token_relay(g).wait_recv()
        else:
            token_near(g).wait_recv()
        a, rows = group(0, g), pl.ds(part * 2 * ROWS, 2 * ROWS)

        @pl.loop(0, 2)
        def _(n):
            wide = pl.ds(pl.multiple_of(n * WIDE, WIDE), WIDE)
            total = jnp.dot(x[a, rows, :], w[0, columns(a), wide], preferred_element_type=F32)
            if g > 0:
                total = total + acc[n, rows, :]
            if g < 7:
                acc[n, rows, :] = total
            else:
                act[rows, wide] = jnp.square(jnp.maximum(total * half_scale[:, wide], 0.0)).astype(BF16)

    def mine(a):
        return acc.at[0, pl.ds(pl.multiple_of((a % 4) * ROWS, ROWS), ROWS), columns(a // 4)]

    def products(first, a, keep):
        @pl.loop(0, 2)
        def _(i):
            rows = pl.ds(pl.multiple_of((first + i) * ROWS, ROWS), ROWS)
            part = lax.dot_general(act[rows, :], w[1, columns(a), :], (((1,), (1,)), ((), ())), preferred_element_type=F32)
            pbuf[keep, i] = part.astype(BF16)
            own[keep % 2, i] = part

    def down_far(g):
        need_group(1, g)
        products(0, group(1, g), 2 * g)
        near_part(g, 0).start()

    def sum_far(g):
        near_part(g, 0).wait_recv()
        zbuf[g] = (own[0, 1] + sibp[g, 0].astype(F32)).astype(BF16)
        far_part(g).start()

    def down_near(g):
        products(2, group(1, g), 2 * g + 1)
        near_part(g, 1).start()

    def output_sum(g):
        near_part(g, 1).wait_recv()
        mine(group(1, g))[...] = own[1, 1] + sibp[g, 1].astype(F32)

    def output(g):
        a = group(1, g, 1)
        far_part(g).wait_recv()
        out[:, columns(a)] = ((mine(a)[...] + zrecv[g].astype(F32)) * down_scale[:, columns(a)]).astype(BF16)

    for step in plan:
        kind, arg = step[0], step[1]
        if kind == 0:
            send(arg, step[2], step[3:6], step[6])
        elif kind == 1:
            token_far_in(arg).wait_recv()
            token_relay(arg).start()
        elif kind == 2:
            up_product(arg, step[2])
        elif kind == 3:
            down_far(arg)
        elif kind == 4:
            sum_far(arg)
        elif kind == 5:
            down_near(arg)
        elif kind == 6:
            output_sum(arg)
        else:
            output(arg)

    for phase in range(2):
        sent = w.at[phase, pl.ds(0, 31 * BLOCK), :]
        remote(sent, sent, ag_send.at[phase], ag_recv.at[0], sibling).wait_send()
    for i in range(3):
        sent = x.at[:, pl.ds(0, ROWS)]
        remote(sent, sent, tok_send.at[i], tok_recv.at[0, 0], sibling).wait_send()
    remote(sibp, sibp, par_send.at[0], par_recv.at[0, 0], sibling).wait_send()
    remote(zbuf, zbuf, par_send.at[1], par_recv.at[0, 0], sibling).wait_send()


def body(hidden_in, norm_gain, up_weight, up_scale, down_weight, down_scale):
    vmem, anywhere = pl.BlockSpec(memory_space=pltpu.VMEM), pl.BlockSpec(memory_space=pl.ANY)
    dma = pltpu.SemaphoreType.DMA
    return pl.pallas_call(
        kernel,
        out_shape=pltpu.VMEM((ROWS, D), BF16),
        in_specs=[anywhere, vmem, anywhere, vmem, anywhere, vmem],
        out_specs=vmem,
        scratch_shapes=[
            pltpu.VMEM((ROWS, D), BF16),
            pltpu.VMEM((BLOCK, Q), F32),
            pltpu.VMEM((BLOCK, Q), F32),
            pltpu.VMEM((2, D, Q), BF16),
            pltpu.VMEM((8, 4 * ROWS, GROUP), BF16),
            pltpu.VMEM((Q // WIDE, 4 * ROWS, WIDE), F32),
            pltpu.VMEM((4 * ROWS, Q), BF16),
            pltpu.VMEM((16, 2, ROWS, GROUP), BF16),
            pltpu.VMEM((8, 2, ROWS, GROUP), BF16),
            pltpu.VMEM((2, 2, ROWS, GROUP), F32),
            pltpu.VMEM((8, ROWS, GROUP), BF16),
            pltpu.VMEM((8, ROWS, GROUP), BF16),
            dma((3,)),
            dma((2,)),
            dma((128,)),
            dma((3,)),
            dma((3, 8)),
            dma((2,)),
            dma((3, 8)),
        ],
        compiler_params=pltpu.CompilerParams(collective_id=0, has_side_effects=True, vmem_limit_bytes=63000000),
        name="ffn",
    )(hidden_in, norm_gain.reshape(1, -1), up_weight, up_scale.reshape(1, -1), down_weight.T, down_scale.reshape(1, -1))


def solution(mesh):
    placed = (P(("rep", "fs", "tp"), None), P(), P("fs", "tp"), P("tp"), P("tp", "fs"), P())
    return jax.shard_map(
        body, mesh=mesh, in_specs=placed, out_specs=P(("rep", "fs", "tp"), None), check_vma=False
    )
```

time: 111 us -> 96.8 us (0.87)
  Pallas kernels: 108 us -> 95.5 us
  local copies, waits for them, and re-layouts: 2.73 us -> 1.15 us
    pallas_call x1, Pallas kernels: 108 us -> 95.5 us  [body(): pl.pallas_call(kernel, out_shape=pltpu.VMEM((ROWS, D), BF16), in_specs=[a...]
    unnamed x1, local copies, waits for them, and re-layouts: 2.73 us -> 1.15 us
where the time goes in v2:
time: 96.8 us; the launch traced here: 96.6 us
  Pallas kernels  95.5 us (99%)
  local copies, waits for them, and re-layouts  1.15 us (1%)
    pallas_call x1, Pallas kernels, body(): pl.pallas_call(kernel, out_shape=pltpu.VMEM((ROWS, D), BF16), in_specs=[a...  95.5 us

profile of v2, /device:TPU:1, one launch (start us, length us, event | category | flops | bytes accessed | tf_op | source)
XLA Modules:
  0.0 96.6 jit_solution(1512197157498888698)
XLA Ops:
  0.0 95.5 %ffn.1 = bf16[384,2048]{1,0:T(8,128)(2,1)S(1)} custom-call(bf16[384,2048]{1,0:T(8,128)(2,1)} %hidden.1, f32[1,2048]{1,0:T(1,128)} %bitcast.6, f32[64,4096]{1,0:T(8,128)} %up.1, f32[1,4096]{1,0:T(1,128)} %bitcast.5, f32[64,4096]{1,0:T(8,128)} %bitcast.4, f32[1,2048]{1,0:T(1,128)} %bitcast.7), custom_call_target="tpu_custom_call" | custom-call | tf_op jit(solution)/shard_map/ffn/pallas_call | solution.py:253
  95.5 1.1 %copy.8 = bf16[384,2048]{1,0:T(8,128)(2,1)} copy(bf16[384,2048]{1,0:T(8,128)(2,1)S(1)} %ffn.1) | data formatting | bytes 3145728

commit v3 on v2

v3 whole, which is shorter than its diff:
```python
import jax
import jax.numpy as jnp
from jax import lax
from jax.experimental import pallas as pl
from jax.experimental.pallas import tpu as pltpu
from jax.sharding import PartitionSpec as P

F32, BF16 = jnp.float32, jnp.bfloat16
ROWS, D, Q, GROUP, BLOCK = 384, 2048, 2048, 256, 64
CHUNKS, WIDE = 2, Q // 2
CHUNK = Q // CHUNKS
STEP = ((1, 0, 0), (3, 0, 0), (0, 1, 0), (0, 3, 0), (0, 0, 1))
ORDER = (
    ((0, 0), (0, 1), (1, 0), (3, 0), (1, 1), (3, 1), (2, 0), (2, 1)),
    ((0, 0), (0, 1), (3, 0), (1, 0), (3, 1), (1, 1), (2, 0), (2, 1)),
)
PLAN = (
    (0,0,0,1,0,0,0), (0,0,0,3,0,0,1), (0,0,1,0,1,0,2), (0,0,0,0,3,0,3), (0,0,1,0,0,1,4), (0,0,1,1,0,0,0),
    (0,1,0,3,0,0,1), (0,0,0,0,1,0,2), (0,0,1,0,3,0,3), (0,0,0,3,0,1,4), (0,1,1,1,0,0,0), (0,0,1,3,1,0,1),
    (0,0,1,0,1,1,2), (0,0,0,1,3,0,3), (0,0,0,0,3,1,4), (0,0,1,2,0,0,0), (0,0,0,3,1,0,1), (0,0,1,1,1,0,2),
    (0,0,1,1,3,0,3), (1,0), (0,0,0,0,1,1,4), (0,0,0,2,3,0,0), (0,0,0,2,0,1,1), (0,0,1,0,2,1,2), (0,0,0,1,2,0,3),
    (1,1), (0,0,1,1,3,1,4), (0,0,1,3,0,0,0), (0,0,0,2,0,0,1), (0,0,0,3,2,0,2), (0,0,1,1,2,0,3), (0,0,1,2,1,0,0),
    (0,1,1,3,0,0,1), (0,0,0,3,3,0,3), (0,0,1,0,3,1,2), (0,0,0,1,2,1,4), (1,2), (0,0,1,0,2,0,4), (0,0,0,1,1,1,0),
    (0,0,0,0,2,0,1), (0,0,0,2,2,0,3), (0,0,1,1,0,1,2), (2,0,0,0), (0,0,1,3,0,1,4), (2,0,1,0), (0,0,1,2,2,0,0),
    (0,0,0,1,0,1,1), (0,0,0,2,1,0,2), (0,0,1,1,2,1,3), (1,3), (0,0,1,2,1,1,4), (0,1,0,1,0,0,0), (0,0,0,0,2,1,1),
    (0,1,1,1,3,0,3), (0,0,1,1,1,1,2), (1,4), (0,0,0,1,1,0,4), (0,0,0,2,1,1,0), (0,0,1,3,2,1,1), (0,0,0,2,3,1,3),
    (0,0,1,3,1,1,2), (0,0,0,2,2,1,4), (0,0,1,3,2,0,0), (0,0,1,2,3,0,2), (0,1,0,0,3,0,3), (1,5), (0,0,0,3,2,1,1),
    (0,0,0,3,3,1,4), (0,1,1,2,3,0,0), (0,1,1,0,3,0,1), (0,0,1,2,2,1,2), (0,0,1,2,0,1,3), (2,2,0,1), (2,2,1,1),
    (0,0,0,3,1,1,0), (0,0,0,1,3,1,1), (0,1,0,1,3,0,3), (0,1,1,1,3,1,4), (1,6), (0,0,1,3,3,0,2), (2,6,1,2),
    (0,0,1,2,3,1,4), (2,6,0,2), (0,1,0,2,0,0,0), (0,1,0,3,3,0,1), (0,0,1,3,3,1,3), (1,7), (0,1,1,2,0,0,2), (2,1,0,3),
    (0,1,1,2,3,1,4), (2,7,0,4), (0,1,1,3,3,0,1), (0,1,1,2,2,0,3), (0,1,1,1,0,1,2), (0,1,0,1,0,1,0), (2,4,0,5),
    (0,1,1,0,3,1,4), (2,3,0,6), (0,1,0,2,3,0,0), (0,1,0,3,0,1,1), (0,1,0,0,1,1,2), (0,1,0,0,3,1,3), (2,5,0,7),
    (0,1,1,3,0,1,1), (0,1,1,0,1,1,2), (0,1,0,1,2,0,3), (0,1,0,2,0,1,4), (3,0), (0,1,1,2,0,1,0), (4,0), (2,7,1,3),
    (0,1,0,3,2,0,3), (0,1,1,3,3,1,4), (2,1,1,4), (0,1,0,1,1,1,0), (0,1,0,3,3,1,1), (0,1,0,0,2,1,2), (3,2),
    (0,1,0,1,3,1,0), (0,1,0,3,1,1,1), (0,1,1,0,2,0,3), (0,1,0,2,3,1,4), (4,2), (0,1,0,2,1,1,2), (2,4,1,5), (3,1),
    (0,1,1,1,1,1,0), (0,1,1,3,1,1,1), (0,1,1,2,1,1,2), (0,1,1,2,2,1,3), (0,1,0,0,1,0,4), (4,1), (2,3,1,6),
    (0,1,0,3,2,1,4), (2,5,1,7), (0,1,1,1,2,0,0), (0,1,0,2,2,0,1), (0,1,1,0,1,0,3), (3,4), (0,1,0,2,2,1,2),
    (0,1,0,1,2,1,3), (0,1,1,0,2,1,4), (0,1,0,0,2,0,0), (0,1,1,3,2,0,1), (4,4), (5,0), (3,5), (0,1,1,3,2,1,0),
    (0,1,0,3,1,0,1), (0,1,1,1,2,1,3), (0,1,1,2,1,0,4), (6,0), (4,5), (5,2), (0,1,0,1,1,0,4), (0,1,0,2,1,0,3), (6,2),
    (5,1), (3,6), (6,1), (7,0), (4,6), (0,1,1,3,1,0,0), (0,1,1,1,1,0,1), (5,4), (3,7), (6,4), (7,2), (4,7), (5,5),
    (7,1), (7,4), (3,3), (6,5), (4,3), (5,6), (6,6), (5,7), (6,7), (5,3), (6,3), (7,5), (7,6), (7,7), (7,3),
)


def kernel(hidden, gain_in, up, up_scale_in, down, down_scale_in, out, gain, up_scale, down_scale, hbuf, ubuf, dbuf, other, w, x, acc, act, pbuf, sibp, own, zbuf, zrecv,
           in_sem, ag_send, ag_recv, tok_send, tok_recv, par_send, par_recv):
    rep, fs, core = lax.axis_index("rep"), lax.axis_index("fs"), lax.axis_index("tp")
    lo, yy, xx = fs // 16, (fs // 4) % 4, fs % 4
    turn = 1 + 2 * core

    def at(px, py, plo):
        return (plo * 4 + py) * 4 + px

    def neighbour(d):
        dx, dy, dz = STEP[d]
        return {"fs": at((xx + turn * dx) % 4, (yy + dy) % 4, (lo + dz) % 2)}

    sibling = {"tp": 1 - core}
    across = {"rep": 1 - rep, "fs": at(xx, yy, 1 - lo)}

    mine_q, far_q = (pl.ds(pl.multiple_of(r * Q, Q), Q) for r in (rep, 1 - rep))
    loads = [
        pltpu.make_async_copy(up.at[:, mine_q], ubuf.at[0], in_sem.at[0]),
        pltpu.make_async_copy(up.at[:, far_q], ubuf.at[1], in_sem.at[1]),
        pltpu.make_async_copy(down.at[:, mine_q], dbuf.at[0], in_sem.at[2]),
        pltpu.make_async_copy(hidden, hbuf, in_sem.at[3]),
        pltpu.make_async_copy(down.at[:, far_q], dbuf.at[1], in_sem.at[4]),
        pltpu.make_async_copy(gain_in, gain, in_sem.at[5]),
        pltpu.make_async_copy(up_scale_in.at[:, mine_q], up_scale, in_sem.at[6]),
        pltpu.make_async_copy(down_scale_in, down_scale, in_sem.at[7]),
    ]
    for load in loads:
        load.start()
    barrier = pltpu.get_barrier_semaphore()
    for peer in [neighbour(d) for d in range(5)] + [sibling, across]:
        pl.semaphore_signal(barrier, inc=1, device_id=peer, device_id_type=pl.DeviceIdType.MESH)

    me_rows = pl.ds(pl.multiple_of(fs * BLOCK, BLOCK), BLOCK)
    loads[0].wait()
    w[0, me_rows, :] = ubuf[0].astype(BF16)
    loads[1].wait()
    other[0] = ubuf[1].astype(BF16)
    loads[2].wait()
    w[1, me_rows, :] = dbuf[0].astype(BF16)
    pl.semaphore_wait(barrier, 7)

    def block_rows(o):
        return pl.ds(pl.multiple_of(at((xx + 4 - (turn * o[0]) % 4) % 4, (yy + 4 - o[1]) % 4, (lo + o[2]) % 2) * BLOCK, BLOCK), BLOCK)

    def remote(src, dst, send, recv, peer):
        return pltpu.make_async_remote_copy(src_ref=src, dst_ref=dst, send_sem=send, recv_sem=recv, device_id=peer,
                                            device_id_type=pl.DeviceIdType.MESH)

    def number(phase, half, o):
        return ((phase * CHUNKS + half) * 2 + o[2]) * 16 + o[1] * 4 + o[0]

    waited = set()

    def send_across(phase):
        for half in range(CHUNKS if phase else CHUNKS // 2):
            part = pl.ds(half * CHUNK, CHUNK)
            remote(other.at[phase, :, part], w.at[phase, me_rows, part], ag_send.at[phase],
                   ag_recv.at[number(phase, half, (0, 0, 1))], across).start()

    def block_copy(phase, half, o, d):
        s = STEP[d]
        held = ((o[0] - s[0]) % 4, (o[1] - s[1]) % 4, (o[2] - s[2]) % 2)
        ref = w.at[phase, block_rows(held), pl.ds(half * CHUNK, CHUNK)]
        return remote(ref, ref, ag_send.at[phase], ag_recv.at[number(phase, half, o)], neighbour(d))

    def need(phase, half, o):
        if o != (0, 0, 0) and (phase, half, o) not in waited:
            waited.add((phase, half, o))
            ref = w.at[phase, block_rows(o), pl.ds(half * CHUNK, CHUNK)]
            remote(ref, ref, ag_send.at[phase], ag_recv.at[number(phase, half, o)], sibling).wait_recv()

    def send(phase, half, o, d):
        s = STEP[d]
        held = ((o[0] - s[0]) % 4, (o[1] - s[1]) % 4, (o[2] - s[2]) % 2)
        need(phase, half, held)
        block_copy(phase, half, o, d).start()

    def need_group(phase, g):
        y, z = ORDER[phase][g]
        for half in range(CHUNKS):
            for a in range(4):
                need(phase, half, (a, y, z))

    def group(phase, g, far=0):
        y, z = ORDER[phase][g]
        return ((lo + far + z) % 2) * 4 + (yy + 4 - y) % 4

    def columns(a):
        return pl.ds(pl.multiple_of(a * GROUP, GROUP), GROUP)

    sib_far_rows, far_rows, sib_rows, my_rows = (pl.ds(i * ROWS, ROWS) for i in range(4))

    def token_far(g):
        a = group(0, g, 1)
        return remote(x.at[a, my_rows], x.at[a, far_rows], tok_send.at[0], tok_recv.at[0, g], across)

    def token_far_in(g):
        a = group(0, g)
        return remote(x.at[a, my_rows], x.at[a, far_rows], tok_send.at[0], tok_recv.at[0, g], across)

    def token_near(g):
        a = group(0, g)
        return remote(x.at[a, my_rows], x.at[a, sib_rows], tok_send.at[1], tok_recv.at[1, g], sibling)

    def token_relay(g):
        a = group(0, g)
        return remote(x.at[a, far_rows], x.at[a, sib_far_rows], tok_send.at[2], tok_recv.at[2, g], sibling)

    def near_part(g, i):
        return remote(pbuf.at[g, i], sibp.at[g, i], par_send.at[0], par_recv.at[i, g], sibling)

    def far_part(g):
        return remote(zbuf.at[g], zrecv.at[g], par_send.at[1], par_recv.at[2, g], across)

    plan = list(PLAN)
    while plan[0][0] == 0 and STEP[plan[0][6]] == tuple(plan[0][3:6]):
        send(plan[0][1], plan[0][2], plan[0][3:6], plan[0][6])
        plan.pop(0)
    send_across(0)
    loads[4].wait()
    other[1] = dbuf[1].astype(BF16)
    loads[3].wait()
    for load in loads[5:]:
        load.wait()

    @pl.loop(0, ROWS // 32)
    def _(i):
        rows = hbuf[pl.ds(i * 32, 32), :].astype(F32)
        inv = lax.rsqrt(jnp.mean(rows * rows, axis=1, keepdims=True) + 1e-06)
        normed = (rows * inv * gain[...]).astype(BF16)
        for a in range(8):
            x[a, pl.ds(3 * ROWS + i * 32, 32), :] = normed[:, a * GROUP:(a + 1) * GROUP]

    for g in range(8):
        token_far(g).start()
    send_across(1)
    for g in range(8):
        token_near(g).start()

    def up_product(g, part, n):
        need_group(0, g)
        if part == 0:
            token_relay(g).wait_recv()
        else:
            token_near(g).wait_recv()
        a, rows = group(0, g), pl.ds(part * 2 * ROWS, 2 * ROWS)

        @pl.loop(0, 2)
        def _(i):
            wide = pl.ds(pl.multiple_of(i * WIDE, WIDE), WIDE)
            total = jnp.dot(x[a, rows, :], w[0, columns(a), wide], preferred_element_type=F32)
            if n > 0:
                total = total + acc[i, rows, :]
            if n < 7:
                acc[i, rows, :] = total
            else:
                act[rows, wide] = jnp.square(jnp.maximum(total * up_scale[:, wide], 0.0)).astype(BF16)

    def mine(a):
        return acc.at[0, pl.ds(pl.multiple_of((a % 4) * ROWS, ROWS), ROWS), columns(a // 4)]

    def products(first, a, g):
        @pl.loop(0, 2)
        def _(i):
            rows = pl.ds(pl.multiple_of((2 * first + i) * ROWS, ROWS), ROWS)
            part = lax.dot_general(act[rows, :], w[1, columns(a), :], (((1,), (1,)), ((), ())), preferred_element_type=F32)
            own[first, i] = part

            @pl.when(i == 0)
            def _():
                pbuf[g, first] = part.astype(BF16)
                near_part(g, first).start()

    def down_far(g):
        need_group(1, g)
        products(0, group(1, g), g)

    def sum_far(g):
        near_part(g, 0).wait_recv()
        zbuf[g] = (own[0, 1] + sibp[g, 0].astype(F32)).astype(BF16)
        far_part(g).start()

    def down_near(g):
        products(1, group(1, g), g)

    def output_sum(g):
        near_part(g, 1).wait_recv()
        mine(group(1, g))[...] = own[1, 1] + sibp[g, 1].astype(F32)

    def output(g):
        a = group(1, g, 1)
        far_part(g).wait_recv()
        out[:, columns(a)] = ((mine(a)[...] + zrecv[g].astype(F32)) * down_scale[:, columns(a)]).astype(BF16)

    for step in plan:
        kind, arg = step[0], step[1]
        if kind == 0:
            send(arg, step[2], step[3:6], step[6])
        elif kind == 1:
            token_far_in(arg).wait_recv()
            token_relay(arg).start()
        elif kind == 2:
            up_product(arg, step[2], step[3])
        elif kind == 3:
            down_far(arg)
        elif kind == 4:
            sum_far(arg)
        elif kind == 5:
            down_near(arg)
        elif kind == 6:
            output_sum(arg)
        else:
            output(arg)

    for phase in range(2):
        sent = w.at[phase, pl.ds(0, 31 * BLOCK), :]
        remote(sent, sent, ag_send.at[phase], ag_recv.at[0], sibling).wait_send()
    for i in range(3):
        sent = x.at[:, pl.ds(0, ROWS)]
        remote(sent, sent, tok_send.at[i], tok_recv.at[0, 0], sibling).wait_send()
    remote(sibp, sibp, par_send.at[0], par_recv.at[0, 0], sibling).wait_send()
    remote(zbuf, zbuf, par_send.at[1], par_recv.at[0, 0], sibling).wait_send()


def body(hidden_in, norm_gain, up_weight, up_scale, down_weight, down_scale):
    vmem, anywhere = pl.BlockSpec(memory_space=pltpu.VMEM), pl.BlockSpec(memory_space=pl.ANY)
    dma = pltpu.SemaphoreType.DMA
    return pl.pallas_call(
        kernel,
        out_shape=pltpu.VMEM((ROWS, D), BF16),
        in_specs=[anywhere] * 6,
        out_specs=vmem,
        scratch_shapes=[
            pltpu.VMEM((1, D), F32),
            pltpu.VMEM((1, Q), F32),
            pltpu.VMEM((1, D), F32),
            pltpu.VMEM((ROWS, D), BF16),
            pltpu.VMEM((2, BLOCK, Q), F32),
            pltpu.VMEM((2, BLOCK, Q), F32),
            pltpu.VMEM((2, BLOCK, Q), BF16),
            pltpu.VMEM((2, D, Q), BF16),
            pltpu.VMEM((8, 4 * ROWS, GROUP), BF16),
            pltpu.VMEM((Q // WIDE, 4 * ROWS, WIDE), F32),
            pltpu.VMEM((4 * ROWS, Q), BF16),
            pltpu.VMEM((8, 2, ROWS, GROUP), BF16),
            pltpu.VMEM((8, 2, ROWS, GROUP), BF16),
            pltpu.VMEM((2, 2, ROWS, GROUP), F32),
            pltpu.VMEM((8, ROWS, GROUP), BF16),
            pltpu.VMEM((8, ROWS, GROUP), BF16),
            dma((8,)),
            dma((2,)),
            dma((CHUNKS * 64,)),
            dma((3,)),
            dma((3, 8)),
            dma((2,)),
            dma((3, 8)),
        ],
        compiler_params=pltpu.CompilerParams(collective_id=0, has_side_effects=True, vmem_limit_bytes=63000000),
        name="ffn",
    )(hidden_in, norm_gain.reshape(1, -1), up_weight, up_scale.reshape(1, -1), down_weight.T, down_scale.reshape(1, -1))


def solution(mesh):
    placed = (P(("rep", "fs", "tp"), None), P(), P("fs", "tp"), P("tp"), P("tp", "fs"), P())
    return jax.shard_map(
        body, mesh=mesh, in_specs=placed, out_specs=P(("rep", "fs", "tp"), None), check_vma=False
    )
```

time: 96.8 us -> 95.1 us (0.982)
  Pallas kernels: 95.5 us -> 93.9 us
    pallas_call x1, Pallas kernels: 95.5 us -> 93.9 us  [body(): pl.pallas_call(kernel, out_shape=pltpu.VMEM((ROWS, D), BF16), in_specs=[a...]
where the time goes in v3:
time: 95.1 us; the launch traced here: 95 us
  Pallas kernels  93.9 us (99%)
  local copies, waits for them, and re-layouts  1.15 us (1%)
    pallas_call x1, Pallas kernels, body(): pl.pallas_call(kernel, out_shape=pltpu.VMEM((ROWS, D), BF16), in_specs=[a...  93.9 us

profile of v3, /device:TPU:1, one launch (start us, length us, event | category | flops | bytes accessed | tf_op | source)
XLA Modules:
  0.0 95.0 jit_solution(5580930857783079743)
XLA Ops:
  0.0 93.9 %ffn.1 = bf16[384,2048]{1,0:T(8,128)(2,1)S(1)} custom-call(bf16[384,2048]{1,0:T(8,128)(2,1)} %hidden.1, f32[1,2048]{1,0:T(1,128)} %bitcast.6, f32[64,4096]{1,0:T(8,128)} %up.1, f32[1,4096]{1,0:T(1,128)} %bitcast.5, f32[64,4096]{1,0:T(8,128)} %bitcast.4, f32[1,2048]{1,0:T(1,128)} %bitcast.7), custom_call_target="tpu_custom_call" | custom-call | tf_op jit(solution)/shard_map/ffn/pallas_call | solution.py:273
  93.9 1.1 %copy.8 = bf16[384,2048]{1,0:T(8,128)(2,1)} copy(bf16[384,2048]{1,0:T(8,128)(2,1)S(1)} %ffn.1) | data formatting | bytes 3145728

commit v4 on v3

--- a/solution.py
+++ b/solution.py
@@ -15,30 +15,30 @@
     ((0, 0), (0, 1), (3, 0), (1, 0), (3, 1), (1, 1), (2, 0), (2, 1)),
 )
 PLAN = (
-    (0,0,0,1,0,0,0), (0,0,0,3,0,0,1), (0,0,1,0,1,0,2), (0,0,0,0,3,0,3), (0,0,1,0,0,1,4), (0,0,1,1,0,0,0),
-    (0,1,0,3,0,0,1), (0,0,0,0,1,0,2), (0,0,1,0,3,0,3), (0,0,0,3,0,1,4), (0,1,1,1,0,0,0), (0,0,1,3,1,0,1),
-    (0,0,1,0,1,1,2), (0,0,0,1,3,0,3), (0,0,0,0,3,1,4), (0,0,1,2,0,0,0), (0,0,0,3,1,0,1), (0,0,1,1,1,0,2),
-    (0,0,1,1,3,0,3), (1,0), (0,0,0,0,1,1,4), (0,0,0,2,3,0,0), (0,0,0,2,0,1,1), (0,0,1,0,2,1,2), (0,0,0,1,2,0,3),
-    (1,1), (0,0,1,1,3,1,4), (0,0,1,3,0,0,0), (0,0,0,2,0,0,1), (0,0,0,3,2,0,2), (0,0,1,1,2,0,3), (0,0,1,2,1,0,0),
-    (0,1,1,3,0,0,1), (0,0,0,3,3,0,3), (0,0,1,0,3,1,2), (0,0,0,1,2,1,4), (1,2), (0,0,1,0,2,0,4), (0,0,0,1,1,1,0),
-    (0,0,0,0,2,0,1), (0,0,0,2,2,0,3), (0,0,1,1,0,1,2), (2,0,0,0), (0,0,1,3,0,1,4), (2,0,1,0), (0,0,1,2,2,0,0),
-    (0,0,0,1,0,1,1), (0,0,0,2,1,0,2), (0,0,1,1,2,1,3), (1,3), (0,0,1,2,1,1,4), (0,1,0,1,0,0,0), (0,0,0,0,2,1,1),
-    (0,1,1,1,3,0,3), (0,0,1,1,1,1,2), (1,4), (0,0,0,1,1,0,4), (0,0,0,2,1,1,0), (0,0,1,3,2,1,1), (0,0,0,2,3,1,3),
-    (0,0,1,3,1,1,2), (0,0,0,2,2,1,4), (0,0,1,3,2,0,0), (0,0,1,2,3,0,2), (0,1,0,0,3,0,3), (1,5), (0,0,0,3,2,1,1),
-    (0,0,0,3,3,1,4), (0,1,1,2,3,0,0), (0,1,1,0,3,0,1), (0,0,1,2,2,1,2), (0,0,1,2,0,1,3), (2,2,0,1), (2,2,1,1),
-    (0,0,0,3,1,1,0), (0,0,0,1,3,1,1), (0,1,0,1,3,0,3), (0,1,1,1,3,1,4), (1,6), (0,0,1,3,3,0,2), (2,6,1,2),
-    (0,0,1,2,3,1,4), (2,6,0,2), (0,1,0,2,0,0,0), (0,1,0,3,3,0,1), (0,0,1,3,3,1,3), (1,7), (0,1,1,2,0,0,2), (2,1,0,3),
-    (0,1,1,2,3,1,4), (2,7,0,4), (0,1,1,3,3,0,1), (0,1,1,2,2,0,3), (0,1,1,1,0,1,2), (0,1,0,1,0,1,0), (2,4,0,5),
-    (0,1,1,0,3,1,4), (2,3,0,6), (0,1,0,2,3,0,0), (0,1,0,3,0,1,1), (0,1,0,0,1,1,2), (0,1,0,0,3,1,3), (2,5,0,7),
-    (0,1,1,3,0,1,1), (0,1,1,0,1,1,2), (0,1,0,1,2,0,3), (0,1,0,2,0,1,4), (3,0), (0,1,1,2,0,1,0), (4,0), (2,7,1,3),
-    (0,1,0,3,2,0,3), (0,1,1,3,3,1,4), (2,1,1,4), (0,1,0,1,1,1,0), (0,1,0,3,3,1,1), (0,1,0,0,2,1,2), (3,2),
-    (0,1,0,1,3,1,0), (0,1,0,3,1,1,1), (0,1,1,0,2,0,3), (0,1,0,2,3,1,4), (4,2), (0,1,0,2,1,1,2), (2,4,1,5), (3,1),
-    (0,1,1,1,1,1,0), (0,1,1,3,1,1,1), (0,1,1,2,1,1,2), (0,1,1,2,2,1,3), (0,1,0,0,1,0,4), (4,1), (2,3,1,6),
-    (0,1,0,3,2,1,4), (2,5,1,7), (0,1,1,1,2,0,0), (0,1,0,2,2,0,1), (0,1,1,0,1,0,3), (3,4), (0,1,0,2,2,1,2),
-    (0,1,0,1,2,1,3), (0,1,1,0,2,1,4), (0,1,0,0,2,0,0), (0,1,1,3,2,0,1), (4,4), (5,0), (3,5), (0,1,1,3,2,1,0),
-    (0,1,0,3,1,0,1), (0,1,1,1,2,1,3), (0,1,1,2,1,0,4), (6,0), (4,5), (5,2), (0,1,0,1,1,0,4), (0,1,0,2,1,0,3), (6,2),
-    (5,1), (3,6), (6,1), (7,0), (4,6), (0,1,1,3,1,0,0), (0,1,1,1,1,0,1), (5,4), (3,7), (6,4), (7,2), (4,7), (5,5),
-    (7,1), (7,4), (3,3), (6,5), (4,3), (5,6), (6,6), (5,7), (6,7), (5,3), (6,3), (7,5), (7,6), (7,7), (7,3),
+    (0,0,0,1,0,0,0), (0,0,0,3,0,0,1), (0,0,0,0,1,0,2), (0,0,1,0,3,0,3), (0,0,1,0,0,1,4), (0,0,1,1,0,0,0),
+    (0,1,0,3,0,0,1), (0,0,1,0,1,0,2), (0,1,1,0,3,0,3), (0,0,0,3,0,1,4), (0,0,1,1,0,1,0), (0,0,1,3,3,0,1),
+    (0,0,0,0,2,0,2), (0,0,1,0,2,0,3), (0,0,1,0,3,1,4), (0,0,1,2,0,0,0), (0,0,0,2,0,0,1), (0,0,0,1,1,0,2),
+    (0,0,1,1,3,0,3), (1,0), (0,0,0,0,2,1,4), (0,0,1,2,0,1,0), (0,0,1,2,3,0,1), (0,0,1,1,1,1,2), (0,0,0,3,3,0,3),
+    (0,0,1,0,2,1,4), (1,1), (0,0,1,3,0,0,0), (0,0,1,3,0,1,1), (0,0,0,1,2,0,2), (0,0,0,2,3,0,3), (0,0,1,1,3,1,0),
+    (0,0,0,2,0,1,1), (0,0,0,0,1,1,2), (0,0,1,3,2,0,3), (0,0,1,1,1,0,4), (0,0,0,3,3,1,4), (1,2), (0,0,0,2,1,0,0),
+    (0,0,0,3,2,1,1), (0,0,1,2,1,1,2), (0,0,1,2,2,0,3), (2,0,0,0), (0,0,0,2,3,1,4), (2,0,1,0), (0,1,1,1,0,0,0),
+    (0,1,1,3,3,0,1), (0,0,1,3,1,0,2), (0,0,1,3,3,1,3), (1,3), (0,0,0,1,2,1,4), (0,0,0,1,1,1,0), (0,0,0,1,0,1,1),
+    (0,0,0,1,3,0,2), (0,0,1,1,2,0,3), (0,0,0,3,2,0,4), (1,4), (0,0,0,3,1,0,0), (0,1,1,3,0,0,1), (0,0,1,3,1,1,2),
+    (0,0,1,2,1,0,3), (0,0,1,2,2,1,4), (0,1,0,1,0,0,0), (0,1,1,2,3,0,1), (0,0,0,2,2,0,2), (0,0,0,3,1,1,3), (1,5),
+    (2,1,0,1), (0,0,0,2,1,1,4), (2,1,1,1), (0,0,0,0,3,0,1), (0,0,1,1,2,1,2), (0,1,0,3,3,0,3), (0,0,1,0,1,1,0),
+    (2,2,0,2), (0,0,0,1,3,1,4), (1,6), (2,2,1,2), (0,0,1,3,2,1,0), (0,1,1,2,0,0,1), (0,0,1,2,3,1,2), (0,0,0,0,3,1,3),
+    (2,6,0,3), (0,0,0,2,2,1,4), (2,6,1,3), (0,1,0,2,0,0,0), (0,1,1,1,3,0,1), (0,1,0,1,1,0,2), (0,1,0,1,3,0,3), (1,7),
+    (2,4,0,4), (0,1,1,3,0,1,4), (2,3,0,5), (0,1,0,0,3,0,0), (0,1,0,2,3,0,1), (0,1,1,0,1,0,2), (0,1,0,3,2,0,3),
+    (2,5,0,6), (0,1,1,2,0,1,4), (0,1,0,1,0,1,0), (0,1,0,3,0,1,1), (0,1,1,2,1,0,2), (0,1,0,0,3,1,3), (2,7,0,7), (3,0),
+    (0,1,1,1,0,1,0), (0,1,0,0,1,0,1), (0,1,0,2,1,0,2), (0,1,1,0,3,1,3), (0,1,0,2,0,1,4), (4,0), (3,2),
+    (0,1,1,1,1,0,0), (0,1,1,3,1,0,1), (0,1,1,0,2,0,2), (0,1,0,3,1,0,3), (0,1,0,2,3,1,4), (4,2), (2,4,1,4), (2,3,1,5),
+    (0,1,0,1,3,1,0), (0,1,0,3,3,1,1), (0,1,0,1,2,0,2), (0,1,1,2,3,1,3), (0,1,0,1,1,1,4), (2,5,1,6), (3,1),
+    (0,1,1,1,3,1,0), (0,1,1,3,3,1,1), (0,1,0,2,2,0,2), (0,1,0,0,2,0,3), (0,1,0,3,2,1,4), (4,1), (2,7,1,7), (3,3),
+    (0,1,1,1,2,0,0), (0,1,1,3,2,0,1), (0,1,1,2,2,0,2), (0,1,1,0,2,1,3), (0,1,1,1,1,1,4), (4,3), (5,0),
+    (0,1,0,2,1,1,0), (0,1,0,0,1,1,1), (0,1,0,3,1,1,2), (0,1,1,2,2,1,3), (0,1,0,1,2,1,4), (6,0), (5,2), (3,4),
+    (0,1,1,3,1,1,2), (0,1,1,1,2,1,3), (0,1,0,0,2,1,4), (6,2), (0,1,1,2,1,1,0), (0,1,1,0,1,1,1), (4,4), (3,6),
+    (0,1,0,2,2,1,4), (4,6), (5,1), (0,1,1,3,2,1,0), (6,1), (5,3), (7,0), (3,5), (6,3), (4,5), (5,4), (3,7), (6,4),
+    (7,2), (4,7), (5,6), (7,1), (6,6), (5,5), (6,5), (5,7), (7,3), (7,4), (6,7), (7,6), (7,5), (7,7),
 )
 
 
@@ -78,10 +78,6 @@
     me_rows = pl.ds(pl.multiple_of(fs * BLOCK, BLOCK), BLOCK)
     loads[0].wait()
     w[0, me_rows, :] = ubuf[0].astype(BF16)
-    loads[1].wait()
-    other[0] = ubuf[1].astype(BF16)
-    loads[2].wait()
-    w[1, me_rows, :] = dbuf[0].astype(BF16)
     pl.semaphore_wait(barrier, 7)
 
     def block_rows(o):
@@ -158,12 +154,15 @@
         return remote(zbuf.at[g], zrecv.at[g], par_send.at[1], par_recv.at[2, g], across)
 
     plan = list(PLAN)
-    while plan[0][0] == 0 and STEP[plan[0][6]] == tuple(plan[0][3:6]):
+    while plan[0][:2] == (0, 0) and STEP[plan[0][6]] == tuple(plan[0][3:6]):
         send(plan[0][1], plan[0][2], plan[0][3:6], plan[0][6])
         plan.pop(0)
+    loads[1].wait()
+    other[0] = ubuf[1].astype(BF16)
     send_across(0)
-    loads[4].wait()
-    other[1] = dbuf[1].astype(BF16)
+    for i, to in ((2, w.at[1, me_rows]), (4, other.at[1])):
+        loads[i].wait()
+        to[...] = dbuf[i // 4].astype(BF16)
     loads[3].wait()
     for load in loads[5:]:
         load.wait()

time: 95.1 us -> 94 us (0.988)
  Pallas kernels: 93.9 us -> 92.7 us
    pallas_call x1, Pallas kernels: 93.9 us -> 92.7 us  [body(): pl.pallas_call(kernel, out_shape=pltpu.VMEM((ROWS, D), BF16), in_specs=[a...]
where the time goes in v4:
time: 94 us; the launch traced here: 93.9 us
  Pallas kernels  92.7 us (99%)
  local copies, waits for them, and re-layouts  1.15 us (1%)
    pallas_call x1, Pallas kernels, body(): pl.pallas_call(kernel, out_shape=pltpu.VMEM((ROWS, D), BF16), in_specs=[a...  92.7 us

profile of v4, /device:TPU:1, one launch (start us, length us, event | category | flops | bytes accessed | tf_op | source)
XLA Modules:
  0.0 93.9 jit_solution(2202338430321292301)
XLA Ops:
  0.0 92.7 %ffn.1 = bf16[384,2048]{1,0:T(8,128)(2,1)S(1)} custom-call(bf16[384,2048]{1,0:T(8,128)(2,1)} %hidden.1, f32[1,2048]{1,0:T(1,128)} %bitcast.6, f32[64,4096]{1,0:T(8,128)} %up.1, f32[1,4096]{1,0:T(1,128)} %bitcast.5, f32[64,4096]{1,0:T(8,128)} %bitcast.4, f32[1,2048]{1,0:T(1,128)} %bitcast.7), custom_call_target="tpu_custom_call" | custom-call | tf_op jit(solution)/shard_map/ffn/pallas_call | solution.py:272
  92.7 1.1 %copy.8 = bf16[384,2048]{1,0:T(8,128)(2,1)} copy(bf16[384,2048]{1,0:T(8,128)(2,1)S(1)} %ffn.1) | data formatting | bytes 3145728

commit v5 on v4

--- a/solution.py
+++ b/solution.py
@@ -15,30 +15,32 @@
     ((0, 0), (0, 1), (3, 0), (1, 0), (3, 1), (1, 1), (2, 0), (2, 1)),
 )
 PLAN = (
-    (0,0,0,1,0,0,0), (0,0,0,3,0,0,1), (0,0,0,0,1,0,2), (0,0,1,0,3,0,3), (0,0,1,0,0,1,4), (0,0,1,1,0,0,0),
-    (0,1,0,3,0,0,1), (0,0,1,0,1,0,2), (0,1,1,0,3,0,3), (0,0,0,3,0,1,4), (0,0,1,1,0,1,0), (0,0,1,3,3,0,1),
-    (0,0,0,0,2,0,2), (0,0,1,0,2,0,3), (0,0,1,0,3,1,4), (0,0,1,2,0,0,0), (0,0,0,2,0,0,1), (0,0,0,1,1,0,2),
-    (0,0,1,1,3,0,3), (1,0), (0,0,0,0,2,1,4), (0,0,1,2,0,1,0), (0,0,1,2,3,0,1), (0,0,1,1,1,1,2), (0,0,0,3,3,0,3),
-    (0,0,1,0,2,1,4), (1,1), (0,0,1,3,0,0,0), (0,0,1,3,0,1,1), (0,0,0,1,2,0,2), (0,0,0,2,3,0,3), (0,0,1,1,3,1,0),
-    (0,0,0,2,0,1,1), (0,0,0,0,1,1,2), (0,0,1,3,2,0,3), (0,0,1,1,1,0,4), (0,0,0,3,3,1,4), (1,2), (0,0,0,2,1,0,0),
-    (0,0,0,3,2,1,1), (0,0,1,2,1,1,2), (0,0,1,2,2,0,3), (2,0,0,0), (0,0,0,2,3,1,4), (2,0,1,0), (0,1,1,1,0,0,0),
-    (0,1,1,3,3,0,1), (0,0,1,3,1,0,2), (0,0,1,3,3,1,3), (1,3), (0,0,0,1,2,1,4), (0,0,0,1,1,1,0), (0,0,0,1,0,1,1),
-    (0,0,0,1,3,0,2), (0,0,1,1,2,0,3), (0,0,0,3,2,0,4), (1,4), (0,0,0,3,1,0,0), (0,1,1,3,0,0,1), (0,0,1,3,1,1,2),
-    (0,0,1,2,1,0,3), (0,0,1,2,2,1,4), (0,1,0,1,0,0,0), (0,1,1,2,3,0,1), (0,0,0,2,2,0,2), (0,0,0,3,1,1,3), (1,5),
-    (2,1,0,1), (0,0,0,2,1,1,4), (2,1,1,1), (0,0,0,0,3,0,1), (0,0,1,1,2,1,2), (0,1,0,3,3,0,3), (0,0,1,0,1,1,0),
-    (2,2,0,2), (0,0,0,1,3,1,4), (1,6), (2,2,1,2), (0,0,1,3,2,1,0), (0,1,1,2,0,0,1), (0,0,1,2,3,1,2), (0,0,0,0,3,1,3),
-    (2,6,0,3), (0,0,0,2,2,1,4), (2,6,1,3), (0,1,0,2,0,0,0), (0,1,1,1,3,0,1), (0,1,0,1,1,0,2), (0,1,0,1,3,0,3), (1,7),
-    (2,4,0,4), (0,1,1,3,0,1,4), (2,3,0,5), (0,1,0,0,3,0,0), (0,1,0,2,3,0,1), (0,1,1,0,1,0,2), (0,1,0,3,2,0,3),
-    (2,5,0,6), (0,1,1,2,0,1,4), (0,1,0,1,0,1,0), (0,1,0,3,0,1,1), (0,1,1,2,1,0,2), (0,1,0,0,3,1,3), (2,7,0,7), (3,0),
-    (0,1,1,1,0,1,0), (0,1,0,0,1,0,1), (0,1,0,2,1,0,2), (0,1,1,0,3,1,3), (0,1,0,2,0,1,4), (4,0), (3,2),
-    (0,1,1,1,1,0,0), (0,1,1,3,1,0,1), (0,1,1,0,2,0,2), (0,1,0,3,1,0,3), (0,1,0,2,3,1,4), (4,2), (2,4,1,4), (2,3,1,5),
-    (0,1,0,1,3,1,0), (0,1,0,3,3,1,1), (0,1,0,1,2,0,2), (0,1,1,2,3,1,3), (0,1,0,1,1,1,4), (2,5,1,6), (3,1),
-    (0,1,1,1,3,1,0), (0,1,1,3,3,1,1), (0,1,0,2,2,0,2), (0,1,0,0,2,0,3), (0,1,0,3,2,1,4), (4,1), (2,7,1,7), (3,3),
-    (0,1,1,1,2,0,0), (0,1,1,3,2,0,1), (0,1,1,2,2,0,2), (0,1,1,0,2,1,3), (0,1,1,1,1,1,4), (4,3), (5,0),
-    (0,1,0,2,1,1,0), (0,1,0,0,1,1,1), (0,1,0,3,1,1,2), (0,1,1,2,2,1,3), (0,1,0,1,2,1,4), (6,0), (5,2), (3,4),
-    (0,1,1,3,1,1,2), (0,1,1,1,2,1,3), (0,1,0,0,2,1,4), (6,2), (0,1,1,2,1,1,0), (0,1,1,0,1,1,1), (4,4), (3,6),
-    (0,1,0,2,2,1,4), (4,6), (5,1), (0,1,1,3,2,1,0), (6,1), (5,3), (7,0), (3,5), (6,3), (4,5), (5,4), (3,7), (6,4),
-    (7,2), (4,7), (5,6), (7,1), (6,6), (5,5), (6,5), (5,7), (7,3), (7,4), (6,7), (7,6), (7,5), (7,7),
+    (0,0,0,1,0,0,0), (0,0,1,3,0,0,1), (0,0,0,0,1,0,2), (0,0,0,0,3,0,3), (0,0,1,0,0,1,4), (0,1,0,1,0,0,0),
+    (0,1,0,3,0,0,1), (0,0,1,0,1,0,2), (0,1,0,0,3,0,3), (0,0,0,1,0,1,4), (0,0,1,1,0,1,0), (0,0,0,3,3,0,1),
+    (0,0,0,1,1,0,2), (0,0,1,3,3,0,3), (0,0,0,0,1,1,4), (0,1,0,1,3,0,0), (0,0,1,2,0,0,1), (0,0,1,0,2,0,2),
+    (0,0,0,0,3,1,3), (1,0), (0,0,0,3,3,1,4), (0,0,1,1,0,0,0), (0,0,0,3,0,1,1), (0,0,1,1,1,1,2), (0,0,0,3,2,0,3),
+    (0,0,0,1,1,1,4), (1,1), (0,0,0,1,3,1,0), (0,0,1,3,0,1,1), (0,0,1,2,1,0,2), (0,0,1,2,3,0,3), (0,0,1,0,2,1,4),
+    (0,1,1,1,0,0,0), (0,1,0,2,0,0,1), (0,0,1,0,1,1,2), (0,0,1,3,2,0,3), (2,0,0,0,1), (2,0,1,0,1), (0,0,0,3,0,0,4),
+    (1,2), (0,0,0,2,0,1,0), (0,0,0,2,2,0,1), (0,0,0,0,2,1,2), (0,0,0,3,1,0,3), (0,0,1,2,1,1,4), (0,0,0,2,3,1,0),
+    (0,0,1,1,1,0,1), (0,0,0,1,2,1,2), (0,0,1,2,2,0,3), (1,3), (0,0,0,1,3,0,4), (0,0,1,1,2,1,0), (0,0,1,1,3,0,1),
+    (0,0,1,3,1,0,2), (0,1,0,2,3,0,3), (2,1,0,0,0), (2,1,1,0,0), (0,0,0,3,1,1,4), (1,4), (0,0,1,2,0,1,0),
+    (0,0,0,2,1,0,1), (0,1,0,1,1,0,2), (0,0,1,3,3,1,3), (2,5,1,1,0), (0,0,0,2,3,0,4), (0,0,1,3,1,1,0),
+    (0,0,1,3,2,1,1), (0,0,1,2,2,1,2), (0,0,0,2,2,1,3), (1,5), (2,2,0,1,1), (2,2,1,1,1), (0,0,0,0,2,0,4), (2,5,0,1,0),
+    (0,1,1,2,0,0,0), (0,0,1,0,3,0,1), (0,0,1,1,3,1,2), (0,0,1,1,2,0,3), (2,1,0,2,1), (2,2,0,2,0), (0,0,0,1,2,0,4),
+    (1,6), (2,1,1,2,1), (0,0,1,0,3,1,0), (0,0,1,2,3,1,1), (0,0,0,3,2,1,2), (0,0,0,2,0,0,3), (2,3,0,3,0), (2,4,0,3,1),
+    (2,2,1,2,0), (0,1,0,3,3,0,1), (0,1,1,0,1,0,2), (0,1,1,1,3,0,3), (0,0,0,2,1,1,4), (2,3,1,3,0), (2,4,1,3,1),
+    (0,1,1,3,0,0,0), (1,7), (2,3,0,4,1), (2,6,0,5,1), (0,1,1,2,0,1,4), (0,1,1,2,1,0,2), (0,1,1,0,3,0,3), (2,7,0,6,1),
+    (2,6,0,4,0), (0,1,0,1,0,1,0), (0,1,0,3,0,1,1), (2,5,0,7,1), (2,7,0,5,0), (0,1,0,3,1,0,2), (0,1,0,1,3,1,4),
+    (2,0,0,6,0), (2,4,0,7,0), (0,1,1,2,3,0,0), (0,1,1,3,0,1,1), (0,1,1,3,3,0,3), (3,0), (0,1,1,3,1,0,2),
+    (0,1,1,0,1,1,4), (4,0), (0,1,1,1,0,1,1), (0,1,1,2,3,1,3), (2,7,1,4,1), (0,1,0,2,0,1,0), (2,3,1,5,1),
+    (0,1,1,0,3,1,4), (2,6,1,6,1), (0,1,1,1,1,0,1), (0,1,0,1,1,1,2), (0,1,0,3,3,1,3), (2,6,1,4,0), (0,1,0,0,1,0,0),
+    (3,2), (0,1,0,3,1,1,4), (0,1,1,0,2,0,2), (0,1,0,2,1,0,1), (4,2), (2,5,1,7,1), (0,1,1,1,1,1,0), (0,1,1,2,2,1,3),
+    (3,1), (0,1,1,3,3,1,4), (0,1,1,3,1,1,2), (0,1,1,1,3,1,1), (0,1,0,2,3,1,3), (4,1), (2,7,1,5,0), (2,0,1,6,0),
+    (0,1,0,0,3,1,0), (2,4,1,7,0), (0,1,0,0,1,1,4), (5,0), (0,1,0,2,1,1,1), (0,1,0,1,2,1,2), (0,1,0,3,2,1,3),
+    (0,1,1,2,1,1,0), (3,3), (0,1,1,0,2,1,4), (6,0), (0,1,1,3,2,0,1), (0,1,0,2,2,0,2), (4,3), (0,1,1,3,2,1,0), (5,2),
+    (0,1,1,1,2,1,3), (3,4), (0,1,0,0,2,0,2), (0,1,1,2,2,0,4), (6,2), (4,4), (5,1), (0,1,0,0,2,1,0), (0,1,0,2,2,1,1),
+    (3,5), (6,1), (7,0), (0,1,0,3,2,0,0), (0,1,0,1,2,0,1), (0,1,1,1,2,0,4), (4,5), (5,3), (6,3), (5,4), (3,7), (6,4),
+    (7,2), (4,7), (5,5), (3,6), (6,5), (7,1), (4,6), (5,7), (7,3), (7,4), (6,7), (5,6), (7,5), (6,6), (7,7), (7,6),
 )
 
 
@@ -90,7 +92,7 @@
     def number(phase, half, o):
         return ((phase * CHUNKS + half) * 2 + o[2]) * 16 + o[1] * 4 + o[0]
 
-    waited = set()
+    waited, fed = set(), set()
 
     def send_across(phase):
         for half in range(CHUNKS if phase else CHUNKS // 2):
@@ -181,22 +183,23 @@
     for g in range(8):
         token_near(g).start()
 
-    def up_product(g, part, n):
-        need_group(0, g)
-        if part == 0:
-            token_relay(g).wait_recv()
-        else:
-            token_near(g).wait_recv()
-        a, rows = group(0, g), pl.ds(part * 2 * ROWS, 2 * ROWS)
+    def up_product(g, part, n, half):
+        y, z = ORDER[0][g]
+        for dx in range(4):
+            need(0, half, (dx, y, z))
+        if (g, part) not in fed:
+            fed.add((g, part))
+            (token_near(g) if part else token_relay(g)).wait_recv()
+        a, wide = group(0, g), pl.ds(half * CHUNK, CHUNK)
 
         @pl.loop(0, 2)
         def _(i):
-            wide = pl.ds(pl.multiple_of(i * WIDE, WIDE), WIDE)
+            rows = pl.ds(pl.multiple_of((2 * part + i) * ROWS, ROWS), ROWS)
             total = jnp.dot(x[a, rows, :], w[0, columns(a), wide], preferred_element_type=F32)
             if n > 0:
-                total = total + acc[i, rows, :]
+                total = total + acc[half, rows, :]
             if n < 7:
-                acc[i, rows, :] = total
+                acc[half, rows, :] = total
             else:
                 act[rows, wide] = jnp.square(jnp.maximum(total * up_scale[:, wide], 0.0)).astype(BF16)
 
@@ -244,7 +247,7 @@
             token_far_in(arg).wait_recv()
             token_relay(arg).start()
         elif kind == 2:
-            up_product(arg, step[2], step[3])
+            up_product(arg, *step[2:])
         elif kind == 3:
             down_far(arg)
         elif kind == 4:

time: 94 us -> 96.3 us (1.024)
  Pallas kernels: 92.7 us -> 95 us
    pallas_call x1, Pallas kernels: 92.7 us -> 95 us  [body(): pl.pallas_call(kernel, out_shape=pltpu.VMEM((ROWS, D), BF16), in_specs=[a...]
where the time goes in v5:
time: 96.3 us; the launch traced here: 96.2 us
  Pallas kernels  95 us (99%)
  local copies, waits for them, and re-layouts  1.15 us (1%)
    pallas_call x1, Pallas kernels, body(): pl.pallas_call(kernel, out_shape=pltpu.VMEM((ROWS, D), BF16), in_specs=[a...  95 us

profile of v5, /device:TPU:1, one launch (start us, length us, event | category | flops | bytes accessed | tf_op | source)
XLA Modules:
  0.0 96.2 jit_solution(8642968719984654936)
XLA Ops:
  0.0 95.0 %ffn.1 = bf16[384,2048]{1,0:T(8,128)(2,1)S(1)} custom-call(bf16[384,2048]{1,0:T(8,128)(2,1)} %hidden.1, f32[1,2048]{1,0:T(1,128)} %bitcast.6, f32[64,4096]{1,0:T(8,128)} %up.1, f32[1,4096]{1,0:T(1,128)} %bitcast.5, f32[64,4096]{1,0:T(8,128)} %bitcast.4, f32[1,2048]{1,0:T(1,128)} %bitcast.7), custom_call_target="tpu_custom_call" | custom-call | tf_op jit(solution)/shard_map/ffn/pallas_call | solution.py:275
  95.0 1.1 %copy.8 = bf16[384,2048]{1,0:T(8,128)(2,1)} copy(bf16[384,2048]{1,0:T(8,128)(2,1)S(1)} %ffn.1) | data formatting | bytes 3145728
